TPU v7x, 32 devices: a whole 2x2x4 slice. The times are simulated.
32 devices in a mesh: kv: 4 (over y, x), tp: 8 (over z, core).
Axes of the slice: x: 2, y: 2, z: 4, core: 2. Of those that a mesh axis runs over, the one named last changes fastest.
Arguments:
- residual: bfloat16 [128, 4096], P(None, ('kv', 'tp')), may hold values from -20 to 20
- mixer_gain: float32 [4096], P('kv'), may hold values from 0.1 to 1.9
- w_query: bfloat16 [4096, 4096], P('kv', 'tp'), may hold values from -0.09375 to 0.09375
- w_forget: bfloat16 [4096, 4096], P('kv', 'tp'), may hold values from -0.09375 to 0.09375
- w_input: bfloat16 [4096, 4096], P('kv', 'tp'), may hold values from -0.09375 to 0.09375
- w_outgate: bfloat16 [4096, 4096], P('kv', 'tp'), may hold values from -0.09375 to 0.09375
- lower_bound: float32 [4096], P('tp'), may hold values from 0.3 to 0.97
- state: float32 [128, 32, 128, 128], P('kv', 'tp'), may hold values from -6 to 6
- head_gain: float32 [128], replicated, may hold values from 0.1 to 1.9
- w_mix_out: bfloat16 [4096, 4096], P('tp', 'kv'), may hold values from -0.09375 to 0.09375
- ffn_gain: float32 [4096], P('kv'), may hold values from 0.1 to 1.9
- w_gate: bfloat16 [4096, 10752], P('kv', 'tp'), may hold values from -0.09375 to 0.09375
- w_up: bfloat16 [4096, 10752], P('kv', 'tp'), may hold values from -0.09375 to 0.09375
- w_down: bfloat16 [10752, 4096], P('tp', 'kv'), may hold values from -0.0625 to 0.0625
Outputs:
- layer_out: bfloat16 [128, 4096], P(None, ('kv', 'tp'))
- new_state: float32 [128, 32, 128, 128], P('kv', 'tp')
All inputs are finite; a program needn't handle non-finite values.
Results may differ from a plain program's by a relative error of at most 0.015.
Values may be sent and summed in bfloat16 or wider, within the bound.
A program may use at most 64 MiB of HBM per device.

v0:
```python
import jax
import jax.numpy as jnp
from jax import lax
from jax.sharding import PartitionSpec as P

D = 4096
DK = 128
DV = 128


EPS = 1e-06


def project_row(weight, piece):
    return jnp.dot(piece, weight, preferred_element_type=jnp.float32)


def channel_mix(rows_in, ffn_gain, w_gate, w_up, w_down):
    rows_float = rows_in.astype(jnp.float32)
    squares = jnp.sum(rows_float * rows_float, axis=1)
    scaled = (rows_float * ffn_gain).astype(jnp.bfloat16)
    gate = jnp.dot(scaled, w_gate, preferred_element_type=jnp.float32)
    upper = jnp.dot(scaled, w_up, preferred_element_type=jnp.float32)
    whole_total = lax.psum(squares, "kv")
    gate, upper = (
        lax.psum(gate.astype(jnp.bfloat16), "kv").astype(jnp.float32),
        lax.psum(upper.astype(jnp.bfloat16), "kv").astype(jnp.float32),
    )
    inverse = lax.rsqrt(whole_total / D + EPS)[:, None]
    hidden = (jax.nn.silu(gate * inverse) * (upper * inverse)).astype(jnp.bfloat16)
    terms = jnp.dot(hidden, w_down, preferred_element_type=jnp.float32)
    summed = lax.psum_scatter(
        terms.astype(jnp.bfloat16), "tp", scatter_dimension=1, tiled=True
    ).astype(jnp.float32)
    width = summed.shape[1]
    own = lax.dynamic_slice_in_dim(rows_float, lax.axis_index("tp") * width, width, 1)
    return (own + summed).astype(jnp.bfloat16)


def body(
    residual,
    mixer_gain,
    w_query,
    w_forget,
    w_input,
    w_outgate,
    lower_bound,
    state,
    head_gain,
    w_mix_out,
    ffn_gain,
    w_gate,
    w_up,
    w_down,
):
    local_seqs, local_heads = (state.shape[0], state.shape[1])
    rows = lax.all_gather(residual, "tp", axis=1, tiled=True)
    rows_float = rows.astype(jnp.float32)
    squares = jnp.sum(rows_float * rows_float, axis=1)
    scaled = (rows_float * mixer_gain).astype(jnp.bfloat16)
    part_query = jnp.dot(scaled, w_query, preferred_element_type=jnp.float32)
    part_forget = jnp.dot(scaled, w_forget, preferred_element_type=jnp.float32)
    part_value = jnp.dot(scaled, w_input, preferred_element_type=jnp.float32)
    part_gate = jnp.dot(scaled, w_outgate, preferred_element_type=jnp.float32)
    whole_total = lax.psum(squares, "kv")
    total = lax.dynamic_slice_in_dim(whole_total, lax.axis_index("kv") * local_seqs, local_seqs)
    part_query, part_forget, part_value, part_gate = (
        lax.psum_scatter(part_query, "kv", scatter_dimension=0, tiled=True),
        lax.psum_scatter(part_forget, "kv", scatter_dimension=0, tiled=True),
        lax.psum_scatter(part_value, "kv", scatter_dimension=0, tiled=True),
        lax.psum_scatter(part_gate, "kv", scatter_dimension=0, tiled=True),
    )
    inverse = lax.rsqrt(total / D + EPS)[:, None]
    bound = lower_bound.reshape(local_heads, DK)
    forget_raw = (part_forget * inverse).reshape(local_seqs, local_heads, DK)
    forget = bound + (1.0 - bound) * jax.nn.sigmoid(forget_raw)
    keyvec = (1.0 - bound) * jax.nn.sigmoid(-forget_raw)
    query = jax.nn.silu((part_query * inverse).reshape(local_seqs, local_heads, DK))
    values = (part_value * inverse).reshape(local_seqs, local_heads, DV)
    updated = forget[..., None] * state + keyvec[..., None] * values[:, :, None, :]
    head_out = jnp.einsum("shc,shce->she", query, updated, precision=lax.Precision.HIGHEST)
    inv_head = lax.rsqrt(jnp.mean(head_out * head_out, axis=2, keepdims=True) + EPS)
    out_gate = jax.nn.silu((part_gate * inverse).reshape(local_seqs, local_heads, DV))
    normed = (
        (head_out * inv_head * head_gain * out_gate)
        .reshape(local_seqs, local_heads * DV)
        .astype(jnp.bfloat16)
    )
    terms = project_row(w_mix_out, lax.all_gather(normed, "kv", axis=0, tiled=True))
    mixed = lax.psum(terms, "tp")
    after_mix = (rows_float + mixed).astype(jnp.bfloat16)
    layer_out = channel_mix(after_mix, ffn_gain, w_gate, w_up, w_down)
    return (layer_out, updated)


def solution(mesh):
    in_specs = (
        P(None, ("kv", "tp")),
        P("kv"),
        P("kv", "tp"),
        P("kv", "tp"),
        P("kv", "tp"),
        P("kv", "tp"),
        P("tp"),
        P("kv", "tp", None, None),
        P(),
        P("tp", "kv"),
        P("kv"),
        P("kv", "tp"),
        P("kv", "tp"),
        P("tp", "kv"),
    )
    out_specs = (P(None, ("kv", "tp")), P("kv", "tp", None, None))
    return jax.shard_map(body, mesh=mesh, in_specs=in_specs, out_specs=out_specs, check_vma=False)
```

profile of v0, /device:TPU:0, one launch (start us, length us, event | category | flops | bytes accessed | tf_op | source)
XLA Modules:
  0.0 312.9 jit_solution(12020792351462122957)
XLA Ops:
  7.2 15.1 %all_gather.6 = bf16[128,1024]{1,0:T(8,128)(2,1)S(1)} all-gather(bf16[128,128]{1,0:T(8,128)(2,1)} %param.14), channel_id=1, replica_groups=mesh['kv'=4,'tp'=8] {'tp'}, dimensions={1}, use_global_device_ids=true | all-gather | bytes 294912 | tf_op jit(solution)/shard_map/all_gather | solution.py:57
  22.4 2.3 fusion.10
  24.7 2.2 fusion.8
  27.0 2.3 fusion.6
  29.4 2.3 fusion.12
  31.7 0.1 fusion.1
  31.8 9.9 %psum.35 = f32[128]{0:T(128)S(1)} all-reduce(f32[128]{0:T(128)S(1)} %fusion.1), channel_id=1, replica_groups=mesh['kv'=4,'tp'=8] {'kv'}, use_global_device_ids=true, to_apply=%region_2.0 | all-reduce | flops 128 | bytes 1024 | tf_op jit(solution)/shard_map/psum | solution.py:65
  41.8 0.1 add_rsqrt_fusion.2
  41.8 0.7 broadcast_subtract_fusion
  42.5 6.5 %reduce-scatter.10.cloned.1.call-done = f32[32,512]{1,0:T(8,128)} async-done(((f32[128,512]{1,0:T(8,128)}), f32[32,512]{1,0:T(8,128)}) %reduce-scatter.10.cloned.1.call-update) | async-done | bytes 65552 | tf_op jit(solution)/shard_map/reduce_scatter | solution.py:69
  49.0 27.1 %reduce-scatter.12.cloned.1.call-done = f32[32,512]{1,0:T(8,128)} async-done(((f32[128,512]{1,0:T(8,128)}), f32[32,512]{1,0:T(8,128)}) %reduce-scatter.12.cloned.1.call-update) | async-done | bytes 65552 | tf_op jit(solution)/shard_map/reduce_scatter | solution.py:70
  76.1 27.2 %reduce-scatter.14.cloned.1.call-done = f32[32,512]{1,0:T(8,128)} async-done(((f32[128,512]{1,0:T(8,128)}), f32[32,512]{1,0:T(8,128)}) %reduce-scatter.14.cloned.1.call-update) | async-done | bytes 65552 | tf_op jit(solution)/shard_map/reduce_scatter | solution.py:71
  103.3 27.0 %reduce-scatter.8.cloned.1.call-done = f32[32,512]{1,0:T(8,128)} async-done(((f32[128,512]{1,0:T(8,128)}), f32[32,512]{1,0:T(8,128)}) %reduce-scatter.8.cloned.1.call-update) | async-done | bytes 65552 | tf_op jit(solution)/shard_map/reduce_scatter | solution.py:68
  130.3 1.0 add_divide_fusion.1
  131.6 8.2 %multiply_add_fusion = f32[32,4,128,128]{3,2,1,0:T(8,128)S(1)} fusion(f32[32,4,128,128]{3,2,1,0:T(8,128)} %param.21, f32[32,4,128]{2,1,0:T(4,128)S(1)} %mul.164, f32[32,4,128]{2,1,0:T(4,128)S(1)} %bitcast.35, f32[32,4,128]{2,1,0:T(4,128)S(1)} %bitcast.34), kind=kLoop, calls=%fused_computation | loop fusion | flops 6291456 | bytes 16973824 | tf_op jit(solution)/shard_map/add | solution.py:80
  139.9 3.4 %copy-done.1 = f32[32,4,128,128]{3,2,1,0:T(8,128)} copy-done((f32[32,4,128,128]{3,2,1,0:T(8,128)}, f32[32,4,128,128]{3,2,1,0:T(8,128)S(1)}, u32[]{:S(2)}) %copy-start.1) | copy-done | bytes 8388632
  143.2 7.2 %fusion.18 = f32[32,4,1,128]{3,2,1,0:T(1,128)S(1)} fusion(f32[32,4,128,1]{2,3,1,0:T(1,128)S(1)} %bitcast.33, f32[32,4,128,128]{3,2,1,0:T(8,128)S(1)} %multiply_add_fusion), kind=kOutput, calls=%fused_computation.39 | convolution fusion | flops 25165824 | bytes 8519680 | tf_op jit(solution)/shard_map/shc,shce->she/dot_general | solution.py:81
  150.5 0.1 multiply_reduce_fusion.1
  150.6 0.1 fusion.15
  150.8 8.5 %all_gather.7 = bf16[128,512]{1,0:T(8,128)(2,1)S(1)} all-gather(bf16[32,512]{1,0:T(8,128)(2,1)S(1)} %bitcast.38), channel_id=1, replica_groups=mesh['kv'=4,'tp'=8] {'kv'}, dimensions={0}, use_global_device_ids=true | all-gather | bytes 163840 | tf_op jit(solution)/shard_map/all_gather | solution.py:89
  159.2 1.1 fusion.19
  160.4 56.7 %all-reduce.4.cloned.1.call-done = f32[128,1024]{1,0:T(8,128)} async-done(((f32[128,1024]{1,0:T(8,128)}), f32[128,1024]{1,0:T(8,128)}) %all-reduce.4.cloned.1.call-update) | async-done | bytes 524304 | tf_op jit(solution)/shard_map/psum | solution.py:90
  217.1 1.2 multiply_reduce_fusion
  218.3 1.6 convolution_convert_fusion
  219.9 3.4 %convolution_convert_fusion.1 = bf16[128,1344]{0,1:T(8,128)(2,1)} fusion(bf16[1024,1344]{0,1:T(8,128)(2,1)} %param.25, f32[128,1024]{1,0:T(8,128)S(1)} %get-tuple-element.5, f32[1024]{0:T(1024)S(1)} %copy-done.3), kind=kOutput, calls=%fused_computation.2 | convolution fusion | flops 352755712 | bytes 3624960 | tf_op jit(solution)/shard_map/dot_general | solution.py:22
  223.4 10.2 %psum.38 = f32[128]{0:T(128)S(1)} all-reduce(f32[128]{0:T(128)S(1)} %get-tuple-element.4), channel_id=1, replica_groups=mesh['kv'=4,'tp'=8] {'kv'}, use_global_device_ids=true, to_apply=%region_10.11 | all-reduce | flops 128 | bytes 1024 | tf_op jit(solution)/shard_map/psum | solution.py:24
  233.6 36.4 %all-reduce.6.cloned.1.call-done = (bf16[128,1344]{0,1:T(8,128)(2,1)}, bf16[128,1344]{0,1:T(8,128)(2,1)}) async-done(((bf16[128,1344]{0,1:T(8,128)(2,1)}, bf16[128,1344]{0,1:T(8,128)(2,1)}), (bf16[128,1344]{0,1:T(8,128)(2,1)}, bf16[128,1344]{0,1:T(8,128)(2,1)})) %all-reduce.6.cloned.1.call-update) | async-done | bytes 688144 | tf_op jit(solution)/shard_map/psum | solution.py:27
  270.0 2.8 convolution_convert_fusion.2
  272.7 0.8 copy.18
  273.6 31.0 %reduce-scatter.16.cloned.1.call-done = bf16[128,128]{1,0:T(8,128)(2,1)} async-done(((bf16[1024,128]{1,0:T(8,128)(2,1)}), bf16[128,128]{1,0:T(8,128)(2,1)}) %reduce-scatter.16.cloned.1.call-update) | async-done | bytes 32784
  304.5 0.9 copy.19
  305.4 0.6 add_convert_fusion
  (37 shorter events, 0.7 us)
Async XLA Ops:
  7.2 211.1 %copy-start = (bf16[1024,1344]{0,1:T(8,128)(2,1)S(1)}, bf16[1024,1344]{0,1:T(8,128)(2,1)}, u32[]{:S(2)}) copy-start(bf16[1024,1344]{0,1:T(8,128)(2,1)} %param.26) | copy-start | bytes 8257540
  7.2 124.4 %copy-start.4 = (f32[512]{0:T(512)S(1)}, f32[512]{0:T(512)}, u32[]{:S(2)}) copy-start(f32[512]{0:T(512)} %param.20) | copy-start | bytes 6148
  7.2 41.8 %reduce-scatter.10.cloned.1.call-start = ((), (), s32[]{:S(2)}) async-start(), calls=%async_computation.6 | async-start | bytes 327680 | tf_op jit(solution)/shard_map/reduce_scatter | solution.py:69
  24.7 51.5 %reduce-scatter.12.cloned.1.call-start = ((), (), s32[]{:S(2)}) async-start(), calls=%async_computation.7 | async-start | bytes 327680 | tf_op jit(solution)/shard_map/reduce_scatter | solution.py:70
  27.0 76.3 %reduce-scatter.14.cloned.1.call-start = ((), (), s32[]{:S(2)}) async-start(), calls=%async_computation.8 | async-start | bytes 327680 | tf_op jit(solution)/shard_map/reduce_scatter | solution.py:71
  29.3 101.0 %reduce-scatter.8.cloned.1.call-start = ((), (), s32[]{:S(2)}) async-start(), calls=%async_computation.5 | async-start | bytes 327680 | tf_op jit(solution)/shard_map/reduce_scatter | solution.py:68
  31.7 185.4 %all-reduce.4.cloned.1.call-start = ((), (), s32[]{:S(2)}) async-start(), calls=%async_computation.9 | async-start | bytes 1048576 | tf_op jit(solution)/shard_map/psum | solution.py:90
  139.8 3.4 %copy-start.1 = (f32[32,4,128,128]{3,2,1,0:T(8,128)}, f32[32,4,128,128]{3,2,1,0:T(8,128)S(1)}, u32[]{:S(2)}) copy-start(f32[32,4,128,128]{3,2,1,0:T(8,128)S(1)} %multiply_add_fusion) | copy-start | bytes 25165828
  139.8 10.8 %copy-start.5 = (f32[128]{0:T(128)S(1)}, f32[128]{0:T(128)}, u32[]{:S(2)}) copy-start(f32[128]{0:T(128)} %param.22) | copy-start | bytes 1540
  139.9 19.4 %copy-start.2 = (bf16[512,1024]{1,0:T(8,128)(2,1)S(1)}, bf16[512,1024]{1,0:T(8,128)(2,1)}, u32[]{:S(2)}) copy-start(bf16[512,1024]{1,0:T(8,128)(2,1)} %param.23) | copy-start | bytes 3145732
  139.9 78.4 %copy-start.3 = (f32[1024]{0:T(1024)S(1)}, f32[1024]{0:T(1024)}, u32[]{:S(2)}) copy-start(f32[1024]{0:T(1024)} %param.24) | copy-start | bytes 12292
  160.4 109.6 %all-reduce.6.cloned.1.call-start = ((), (), s32[]{:S(2)}) async-start(), calls=%async_computation.11 | async-start | bytes 1376256 | tf_op jit(solution)/shard_map/psum | solution.py:27
  223.4 81.2 %reduce-scatter.16.cloned.1.call-start = ((), (), s32[]{:S(2)}) async-start(), calls=%async_computation.10 | async-start | bytes 294912
Sparse Core Ops, SparseCore 0:
  24.8 24.1 reduce-scatter.9
  51.7 24.3 reduce-scatter.11
  78.9 24.3 reduce-scatter.13
  105.9 24.3 reduce-scatter.7
  160.5 56.5 all-reduce.3
  223.5 46.4 all-reduce.5
  273.7 30.7 reduce-scatter.15
where the time goes:
time: 314 us; the launch traced here: 313 us
  waiting for transfers between devices  212 us (68%)
  blocking collectives  43.7 us (14%)
  matrix products  25.2 us (8%)
  between operations  14.3 us (5%)
  other arithmetic  12.3 us (4%)
  local copies, waits for them, and re-layouts  5.22 us (2%)
    psum x1, waiting for transfers between devices, body(): mixed = lax.psum(terms, 'tp')  56.7 us
    psum x1, waiting for transfers between devices, channel_mix(): lax.psum(upper.astype(jnp.bfloat16), 'kv').astype(jnp.float32)  36.4 us
    unnamed x8, waiting for transfers between devices  31.1 us
    reduce_scatter x1, waiting for transfers between devices, body(): lax.psum_scatter(part_gate, 'kv', scatter_dimension=0, tiled=True)  27.2 us
    reduce_scatter x1, waiting for transfers between devices, body(): lax.psum_scatter(part_value, 'kv', scatter_dimension=0, tiled=True)  27.1 us
    reduce_scatter x1, waiting for transfers between devices, body(): lax.psum_scatter(part_query, 'kv', scatter_dimension=0, tiled=True)  27 us
    all_gather x1, blocking collectives, body(): rows = lax.all_gather(residual, 'tp', axis=1, tiled=True)  15.1 us
    psum x1, blocking collectives, channel_mix(): whole_total = lax.psum(squares, 'kv')  10.2 us
  transfers between devices with their start and end apart: 7, of which 7 were waited for; matrix products, arithmetic and copies ran while one was open for 2% of the time, Pallas kernels for 0%

commit v1 on v0

v1 whole, which is shorter than its diff:
```python
import functools

import jax
import jax.numpy as jnp
from jax import lax
from jax.experimental import pallas as pl
from jax.experimental.pallas import tpu as pltpu
from jax.sharding import PartitionSpec as P

EPS = 1e-06
F32 = jnp.float32
BF16 = jnp.bfloat16
LANES = 128


def ring(axis, size):
    me = lax.axis_index(axis)
    return me, [lax.rem(me + step, size) for step in range(1, size)]


def greet(axes):
    barrier = pltpu.get_barrier_semaphore()
    count = 0
    for axis, peers in axes:
        for peer in peers:
            pl.semaphore_signal(
                barrier, inc=1, device_id={axis: peer}, device_id_type=pl.DeviceIdType.MESH
            )
            count += 1
    pl.semaphore_wait(barrier, count)


def remote(source, target, send_sem, recv_sem, axis, peer):
    return pltpu.make_async_remote_copy(
        src_ref=source,
        dst_ref=target,
        send_sem=send_sem,
        recv_sem=recv_sem,
        device_id={axis: peer},
        device_id_type=pl.DeviceIdType.MESH,
    )


def scale_block(blocks, gain_ref, scaled, count, width):
    squares = None
    for j in range(count):
        rows = blocks[j].astype(F32)
        cols = slice(j * width, (j + 1) * width)
        scaled[:, cols] = (rows * gain_ref[:, cols]).astype(BF16)
        term = rows * rows
        squares = term if squares is None else squares + term
    total = jnp.sum(squares, axis=1, keepdims=True)
    return jnp.broadcast_to(total, (total.shape[0], LANES))


def project_kernel(
    n_kv, n_tp, features,
    x_ref, gain_ref, wq, wf, wi, wo,
    out_ref,
    weights, blocks, scaled, parts, landed, squares, squares_in,
    w_sem, x_send, x_recv, p_send, p_recv, s_send, s_recv,
):
    seqs, width = x_ref.shape
    local = out_ref.shape[1]
    loads = [
        pltpu.make_async_copy(source, weights.at[i], w_sem.at[i])
        for i, source in enumerate((wq, wf, wi, wo))
    ]
    for load in loads:
        load.start()
    kv, kv_peers = ring("kv", n_kv)
    tp, tp_peers = ring("tp", n_tp)
    greet((("kv", kv_peers), ("tp", tp_peers)))

    gathers = [
        remote(x_ref, blocks.at[tp], x_send.at[i], x_recv.at[i], "tp", peer)
        for i, peer in enumerate(tp_peers)
    ]
    for copy in gathers:
        copy.start()
    blocks[pl.ds(tp, 1)] = x_ref[...][None]
    for copy in gathers:
        copy.wait_recv()
    squares[...] = scale_block(blocks, gain_ref, scaled, n_tp, width)
    square_copies = [
        remote(
            squares.at[pl.ds(pl.multiple_of(peer * local, local), local), :],
            squares_in.at[i], s_send.at[i], s_recv.at[i], "kv", peer,
        )
        for i, peer in enumerate(kv_peers)
    ]
    for copy in square_copies:
        copy.start()
    for load in loads:
        load.wait()
    part_copies = []
    for p in range(4):
        parts[p] = jnp.dot(scaled[...], weights[p], preferred_element_type=F32).astype(BF16)
        for i, peer in enumerate(kv_peers):
            copy = remote(
                parts.at[p, pl.ds(pl.multiple_of(peer * local, local), local), :],
                landed.at[i, p], p_send.at[i, p], p_recv.at[i, p], "kv", peer,
            )
            copy.start()
            part_copies.append(copy)
    own = pl.ds(pl.multiple_of(kv * local, local), local)
    total = squares[own, :]
    for copy in square_copies:
        copy.wait_recv()
    for i in range(n_kv - 1):
        total = total + squares_in[i]
    inverse = lax.rsqrt(total[:, :1] / features + EPS)
    for copy in part_copies:
        copy.wait_recv()
    for p in range(4):
        value = parts[p, own, :].astype(F32)
        for i in range(n_kv - 1):
            value = value + landed[i, p].astype(F32)
        out_ref[p] = value * inverse
    for copy in gathers + square_copies + part_copies:
        copy.wait_send()


def state_kernel(q_ref, f_ref, v_ref, g_ref, bound_ref, gain_ref, state_ref, new_ref, normed_ref):
    rows = q_ref.shape[1]
    bound = bound_ref[...]
    raw = f_ref[0]
    forget = bound + (1.0 - bound) * jax.nn.sigmoid(raw)
    keyvec = (1.0 - bound) * jax.nn.sigmoid(-raw)
    query = q_ref[0] * jax.nn.sigmoid(q_ref[0])
    forget_t, keyvec_t, query_t = forget.T, keyvec.T, query.T
    for s in range(rows):
        new = (
            forget_t[:, s : s + 1] * state_ref[s, 0]
            + keyvec_t[:, s : s + 1] * v_ref[0, s : s + 1, :]
        )
        new_ref[s, 0] = new
        head = jnp.sum(query_t[:, s : s + 1] * new, axis=0, keepdims=True)
        inverse = lax.rsqrt(jnp.mean(head * head, axis=1, keepdims=True) + EPS)
        gate = g_ref[0, s : s + 1, :]
        normed_ref[s : s + 1, :] = head * inverse * gain_ref[...] * (gate * jax.nn.sigmoid(gate))


def mix_kernel(
    n_kv, n_tp, features,
    normed_ref, x_ref, gain_ref, w_mix, w_gate, w_up, w_down,
    out_ref,
    mix_w, gate_w, down_w, normed16, heads, terms, terms_in, mixed, blocks, scaled,
    squares, squares_in, parts, landed, hidden, hiddens, downs, downs_in,
    w_sem, n_send, n_recv, t_send, t_recv, m_send, m_recv, s_send, s_recv,
    g_send, g_recv, h_send, h_recv, d_send, d_recv,
):
    seqs, width = x_ref.shape
    local = normed_ref.shape[0]
    units = gate_w.shape[1]
    loads = [
        pltpu.make_async_copy(source, target, w_sem.at[i])
        for i, (source, target) in enumerate(
            ((w_mix, mix_w), (w_gate, gate_w.at[0]), (w_up, gate_w.at[1]), (w_down, down_w))
        )
    ]
    for load in loads:
        load.start()
    normed16[...] = normed_ref[...].astype(BF16)
    kv, kv_peers = ring("kv", n_kv)
    tp, tp_peers = ring("tp", n_tp)
    own = pl.ds(pl.multiple_of(kv * local, local), local)
    greet((("kv", kv_peers), ("tp", tp_peers)))

    pending = []
    copies = [
        remote(normed16, heads.at[own, :], n_send.at[i], n_recv.at[i], "kv", peer)
        for i, peer in enumerate(kv_peers)
    ]
    for copy in copies:
        copy.start()
    pending += copies
    heads[own, :] = normed16[...]
    loads[0].wait()
    for copy in copies:
        copy.wait_recv()

    group = max(1, 256 // width)
    while n_tp % group:
        group -= 1

    def scatter(left, weight, sums, sums_in, send, recv):
        for t in range(0, n_tp, group):
            part = jnp.dot(
                left[...], weight[:, t * width : (t + group) * width], preferred_element_type=F32
            ).astype(BF16)
            for j in range(group):
                sums[t + j] = part[:, j * width : (j + 1) * width]
        out = [
            remote(sums.at[peer], sums_in.at[i], send.at[i], recv.at[i], "tp", peer)
            for i, peer in enumerate(tp_peers)
        ]
        for copy in out:
            copy.start()
        return out

    def collect(base, sums, sums_in, out):
        total = base + sums[pl.ds(tp, 1)][0].astype(F32)
        for copy in out:
            copy.wait_recv()
        for i in range(n_tp - 1):
            total = total + sums_in[i].astype(F32)
        return total.astype(BF16)

    copies = scatter(heads, mix_w, terms, terms_in, t_send, t_recv)
    pending += copies
    mixed[...] = collect(x_ref[...].astype(F32), terms, terms_in, copies)

    copies = [
        remote(mixed, blocks.at[tp], m_send.at[i], m_recv.at[i], "tp", peer)
        for i, peer in enumerate(tp_peers)
    ]
    for copy in copies:
        copy.start()
    pending += copies
    blocks[pl.ds(tp, 1)] = mixed[...][None]
    for copy in copies:
        copy.wait_recv()
    squares[...] = scale_block(blocks, gain_ref, scaled, n_tp, width)
    square_copies = [
        remote(
            squares.at[pl.ds(pl.multiple_of(peer * local, local), local), :],
            squares_in.at[i], s_send.at[i], s_recv.at[i], "kv", peer,
        )
        for i, peer in enumerate(kv_peers)
    ]
    for copy in square_copies:
        copy.start()
    pending += square_copies

    copies = []
    step = min(512, units)
    for g in range(2):
        loads[1 + g].wait()
        for c in range(0, units, step):
            end = min(c + step, units)
            parts[g, :, c:end] = lax.dot_general(
                scaled[...], gate_w[g, c:end, :], (((1,), (1,)), ((), ())),
                preferred_element_type=F32,
            ).astype(BF16)
        for i, peer in enumerate(kv_peers):
            copy = remote(
                parts.at[g, pl.ds(pl.multiple_of(peer * local, local), local), :],
                landed.at[i, g], g_send.at[i, g], g_recv.at[i, g], "kv", peer,
            )
            copy.start()
            copies.append(copy)
    pending += copies
    for copy in square_copies:
        copy.wait_recv()
    total = squares[own, :]
    for i in range(n_kv - 1):
        total = total + squares_in[i]
    inverse = lax.rsqrt(total[:, :1] / features + EPS)
    for copy in copies:
        copy.wait_recv()
    sums = []
    for g in range(2):
        value = parts[g, own, :].astype(F32)
        for i in range(n_kv - 1):
            value = value + landed[i, g].astype(F32)
        sums.append(value * inverse)
    hidden[...] = (sums[0] * jax.nn.sigmoid(sums[0]) * sums[1]).astype(BF16)

    copies = [
        remote(hidden, hiddens.at[own, :], h_send.at[i], h_recv.at[i], "kv", peer)
        for i, peer in enumerate(kv_peers)
    ]
    for copy in copies:
        copy.start()
    pending += copies
    hiddens[own, :] = hidden[...]
    loads[3].wait()
    for copy in copies:
        copy.wait_recv()
    copies = scatter(hiddens, down_w, downs, downs_in, d_send, d_recv)
    pending += copies
    out_ref[...] = collect(mixed[...].astype(F32), downs, downs_in, copies)
    for copy in pending:
        copy.wait_send()


def in_vmem():
    return pl.BlockSpec(memory_space=pltpu.VMEM)


def in_hbm():
    return pl.BlockSpec(memory_space=pl.ANY)


def body(
    n_kv, n_tp,
    residual, mixer_gain, w_query, w_forget, w_input, w_outgate, lower_bound, state,
    head_gain, w_mix_out, ffn_gain, w_gate, w_up, w_down,
):
    seqs, width = residual.shape
    depth, hid = w_query.shape
    local, heads, dk, dv = state.shape
    units = w_gate.shape[1]
    features = depth * n_kv
    dma = pltpu.SemaphoreType.DMA

    raw = pl.pallas_call(
        functools.partial(project_kernel, n_kv, n_tp, features),
        out_shape=jax.ShapeDtypeStruct((4, local, hid), F32),
        in_specs=[in_vmem()] * 2 + [in_hbm()] * 4,
        out_specs=in_vmem(),
        scratch_shapes=[
            pltpu.VMEM((4, depth, hid), BF16),
            pltpu.VMEM((n_tp, seqs, width), BF16),
            pltpu.VMEM((seqs, depth), BF16),
            pltpu.VMEM((4, seqs, hid), BF16),
            pltpu.VMEM((n_kv - 1, 4, local, hid), BF16),
            pltpu.VMEM((seqs, LANES), F32),
            pltpu.VMEM((n_kv - 1, local, LANES), F32),
            dma((4,)),
            dma((n_tp - 1,)), dma((n_tp - 1,)),
            dma((n_kv - 1, 4)), dma((n_kv - 1, 4)),
            dma((n_kv - 1,)), dma((n_kv - 1,)),
        ],
        compiler_params=pltpu.CompilerParams(collective_id=0, has_side_effects=True),
        name="project",
    )(residual, mixer_gain.reshape(1, depth), w_query, w_forget, w_input, w_outgate)

    rows = 16 if local % 16 == 0 else local
    pick = lambda p: pl.BlockSpec((1, rows, dk), lambda h, s: (p, s, h))
    updated, normed = pl.pallas_call(
        state_kernel,
        grid=(heads, local // rows),
        out_shape=(
            jax.ShapeDtypeStruct(state.shape, F32),
            jax.ShapeDtypeStruct((local, heads * dv), F32),
        ),
        in_specs=[
            pick(0), pick(1), pick(2), pick(3),
            pl.BlockSpec((1, dk), lambda h, s: (0, h)),
            pl.BlockSpec((1, dv), lambda h, s: (0, 0)),
            pl.BlockSpec((rows, 1, dk, dv), lambda h, s: (s, h, 0, 0)),
        ],
        out_specs=(
            pl.BlockSpec((rows, 1, dk, dv), lambda h, s: (s, h, 0, 0)),
            pl.BlockSpec((rows, dv), lambda h, s: (s, h)),
        ),
        name="state",
    )(raw, raw, raw, raw, lower_bound.reshape(1, hid), head_gain.reshape(1, dv), state)

    layer_out = pl.pallas_call(
        functools.partial(mix_kernel, n_kv, n_tp, features),
        out_shape=jax.ShapeDtypeStruct((seqs, width), BF16),
        in_specs=[in_vmem()] * 3 + [in_hbm()] * 4,
        out_specs=in_vmem(),
        scratch_shapes=[
            pltpu.VMEM(w_mix_out.shape, BF16),
            pltpu.VMEM((2, units, depth), BF16),
            pltpu.VMEM(w_down.shape, BF16),
            pltpu.VMEM((local, hid), BF16),
            pltpu.VMEM((seqs, hid), BF16),
            pltpu.VMEM((n_tp, seqs, width), BF16),
            pltpu.VMEM((n_tp - 1, seqs, width), BF16),
            pltpu.VMEM((seqs, width), BF16),
            pltpu.VMEM((n_tp, seqs, width), BF16),
            pltpu.VMEM((seqs, depth), BF16),
            pltpu.VMEM((seqs, LANES), F32),
            pltpu.VMEM((n_kv - 1, local, LANES), F32),
            pltpu.VMEM((2, seqs, units), BF16),
            pltpu.VMEM((n_kv - 1, 2, local, units), BF16),
            pltpu.VMEM((local, units), BF16),
            pltpu.VMEM((seqs, units), BF16),
            pltpu.VMEM((n_tp, seqs, width), BF16),
            pltpu.VMEM((n_tp - 1, seqs, width), BF16),
            dma((4,)),
            dma((n_kv - 1,)), dma((n_kv - 1,)),
            dma((n_tp - 1,)), dma((n_tp - 1,)),
            dma((n_tp - 1,)), dma((n_tp - 1,)),
            dma((n_kv - 1,)), dma((n_kv - 1,)),
            dma((n_kv - 1, 2)), dma((n_kv - 1, 2)),
            dma((n_kv - 1,)), dma((n_kv - 1,)),
            dma((n_tp - 1,)), dma((n_tp - 1,)),
        ],
        compiler_params=pltpu.CompilerParams(collective_id=1, has_side_effects=True),
        name="mix",
    )(normed, residual, ffn_gain.reshape(1, depth), w_mix_out, w_gate.T, w_up.T, w_down)
    return layer_out, updated


def solution(mesh):
    in_specs = (
        P(None, ("kv", "tp")),
        P("kv"),
        P("kv", "tp"),
        P("kv", "tp"),
        P("kv", "tp"),
        P("kv", "tp"),
        P("tp"),
        P("kv", "tp", None, None),
        P(),
        P("tp", "kv"),
        P("kv"),
        P("kv", "tp"),
        P("kv", "tp"),
        P("tp", "kv"),
    )
    out_specs = (P(None, ("kv", "tp")), P("kv", "tp", None, None))
    return jax.shard_map(
        functools.partial(body, mesh.shape["kv"], mesh.shape["tp"]),
        mesh=mesh, in_specs=in_specs, out_specs=out_specs, check_vma=False,
    )
```

time: 314 us -> 89.2 us (0.28)
  waiting for transfers between devices: 212 us -> 0 us
  Pallas kernels: 0 us -> 86.3 us
  blocking collectives: 43.7 us -> 0 us
  matrix products: 25.2 us -> 0 us
  between operations: 14.3 us -> 0.65 us
  other arithmetic: 12.3 us -> 0 us
  local copies, waits for them, and re-layouts: 5.22 us -> 1.38 us
    psum x2 -> x0, waiting for transfers between devices: 93 us -> none  [the longest x1 56.7 us: body(): mixed = lax.psum(terms, 'tp')]
    reduce_scatter x4 -> x0, waiting for transfers between devices: 87.8 us -> none  [the longest x1 27.2 us: body(): lax.psum_scatter(part_gate, 'kv', scatter_dimension=0, tiled=True)]
    pallas_call x0 -> x3, Pallas kernels: none -> 86.3 us  [the longest x1 44.8 us: body(): pl.pallas_call(functools.partial(mix_kernel, n_kv, n_tp, features), out_s...]
    unnamed x8 -> x0, waiting for transfers between devices: 31.1 us -> none
    dot_general x9 -> x0, matrix products: 25.2 us -> none  [the longest x1 7.25 us: body(): jnp.einsum('shc,shce->she', query, updated, precision=lax.Precision.HIGHEST)]
    all_gather x2 -> x0, blocking collectives: 23.6 us -> none  [the longest x1 15.1 us: body(): rows = lax.all_gather(residual, 'tp', axis=1, tiled=True)]
    psum x2 -> x0, blocking collectives: 20.1 us -> none  [the longest x1 10.2 us: channel_mix(): whole_total = lax.psum(squares, 'kv')]
    add x2 -> x0, other arithmetic: 8.24 us -> none  [the longest x1 8.22 us: body(): forget[..., None] * state + keyvec[..., None] * values[:, :, None, :]]
  transfers between devices with their start and end apart: 7 -> 0, of which waited for: 7 -> 0; matrix products, arithmetic and copies ran while one was open for 2% -> 0% of each run, Pallas kernels for 0% -> 0%
where the time goes in v1:
time: 89.2 us; the launch traced here: 88.3 us
  Pallas kernels  86.3 us (97%)
  local copies, waits for them, and re-layouts  1.38 us (2%)
    pallas_call x1, Pallas kernels, body(): pl.pallas_call(functools.partial(mix_kernel, n_kv, n_tp, features), out_s...  44.8 us
    pallas_call x1, Pallas kernels, body(): pl.pallas_call(functools.partial(project_kernel, n_kv, n_tp, features), o...  22 us
    pallas_call x1, Pallas kernels, body(): pl.pallas_call(state_kernel, grid=(heads, local // rows), out_shape=(jax....  19.5 us

profile of v1, /device:TPU:0, one launch (start us, length us, event | category | flops | bytes accessed | tf_op | source)
XLA Modules:
  0.0 88.3 jit_solution(206491186530871692)
XLA Ops:
  0.6 22.0 %project.1.q_ref.f_ref.v_ref.g_ref = f32[4,32,512]{2,1,0:T(8,128)} custom-call(bf16[128,128]{1,0:T(8,128)(2,1)} %x_ref.3, f32[1,1024]{1,0:T(1,128)} %bitcast.8, bf16[1024,512]{1,0:T(8,128)(2,1)} %wq.1, bf16[1024,512]{1,0:T(8,128)(2,1)} %wf.1, bf16[1024,512]{1,0:T(8,128)(2,1)} %wi.1, bf16[1024,512]{1,0:T(8,128)(2,1)} %wo.1), custom_call_target="tpu_custom_call" | custom-call | tf_op jit(solution)/shard_map/project/pallas_call | solution.py:308
  22.6 19.5 %state.1 = (f32[32,4,128,128]{3,2,1,0:T(8,128)}, f32[32,512]{1,0:T(8,128)}) custom-call(f32[4,32,512]{2,1,0:T(8,128)} %project.1.q_ref.f_ref.v_ref.g_ref, f32[4,32,512]{2,1,0:T(8,128)} %project.1.q_ref.f_ref.v_ref.g_ref, f32[4,32,512]{2,1,0:T(8,128)} %project.1.q_ref.f_ref.v_ref.g_ref, f32[4,32,512]{2,1,0:T(8,128)} %project.1.q_ref.f_ref.v_ref.g_ref, ...), custom_call_target="tpu_custom_call" | custom-call | tf_op jit(solution)/shard_map/state/pallas_call | solution.py:332
  42.1 44.8 %mix.1 = bf16[128,128]{1,0:T(8,128)(2,1)} custom-call(f32[32,512]{1,0:T(8,128)} %get-tuple-element.4.normed_ref, bf16[128,128]{1,0:T(8,128)(2,1)} %x_ref.3, f32[1,1024]{1,0:T(1,128)} %bitcast.9, bf16[512,1024]{1,0:T(8,128)(2,1)} %w_mix.1, bf16[1344,1024]{1,0:T(8,128)(2,1)} %bitcast.6, bf16[1344,1024]{1,0:T(8,128)(2,1)} %bitcast.7, bf16[1344,1024]{1,0:T(8,128)(2,1)} %w_down.1), custom_call_target="tpu_custom_call" | custom-call | tf_op jit(solution)/shard_map/mix/pallas_call | solution.py:352
  86.9 1.4 %copy.17 = bf16[128,128]{1,0:T(8,128)(2,1)} copy(bf16[128,128]{1,0:T(8,128)(2,1)} %mix.1) | data formatting | bytes 65536

commit v2 on v1

--- a/solution.py
+++ b/solution.py
@@ -39,6 +39,41 @@
         device_id={axis: peer},
         device_id_type=pl.DeviceIdType.MESH,
     )
+
+
+def pairs(n_tp):
+    me = lax.axis_index("tp")
+    core = lax.rem(me, 2)
+    return me, core, lax.div(me, 2), me + 1 - 2 * core, n_tp // 2
+
+
+def gather_pairs(n_tp, source, blocks, send, recv):
+    me, _, _, partner, half = pairs(n_tp)
+    peers = [lax.rem(me + 2 * i, n_tp) for i in range(1, half)]
+    origins = [lax.rem(me - 2 * i + n_tp, n_tp) for i in range(1, half)]
+    direct = [
+        remote(source, blocks.at[me], send.at[i], recv.at[i], "tp", peer)
+        for i, peer in enumerate(peers)
+    ]
+    direct.append(
+        remote(source, blocks.at[me], send.at[half - 1], recv.at[half - 1], "tp", partner)
+    )
+    for copy in direct:
+        copy.start()
+    blocks[pl.ds(me, 1)] = source[...][None]
+    relays = []
+    for i, origin in enumerate(origins):
+        direct[i].wait_recv()
+        relay = remote(
+            blocks.at[origin], blocks.at[origin],
+            send.at[half + i], recv.at[half + i], "tp", partner,
+        )
+        relay.start()
+        relays.append(relay)
+    direct[-1].wait_recv()
+    for relay in relays:
+        relay.wait_recv()
+    return direct + relays
 
 
 def scale_block(blocks, gain_ref, scaled, count, width):
@@ -70,17 +105,10 @@
         load.start()
     kv, kv_peers = ring("kv", n_kv)
     tp, tp_peers = ring("tp", n_tp)
-    greet((("kv", kv_peers), ("tp", tp_peers)))
-
-    gathers = [
-        remote(x_ref, blocks.at[tp], x_send.at[i], x_recv.at[i], "tp", peer)
-        for i, peer in enumerate(tp_peers)
-    ]
-    for copy in gathers:
-        copy.start()
-    blocks[pl.ds(tp, 1)] = x_ref[...][None]
-    for copy in gathers:
-        copy.wait_recv()
+    near = pairs(n_tp)[3]
+    greet((("kv", kv_peers), ("tp", [near] + tp_peers[1::2])))
+
+    gathers = gather_pairs(n_tp, x_ref, blocks, x_send, x_recv)
     squares[...] = scale_block(blocks, gain_ref, scaled, n_tp, width)
     square_copies = [
         remote(
@@ -121,32 +149,48 @@
         copy.wait_send()
 
 
-def state_kernel(q_ref, f_ref, v_ref, g_ref, bound_ref, gain_ref, state_ref, new_ref, normed_ref):
-    rows = q_ref.shape[1]
+def split(value):
+    high = value.astype(BF16).astype(F32)
+    return high, value - high
+
+
+def state_kernel(q_ref, f_ref, v_ref, g_ref, bound_ref, gain_ref, state_ref, new_ref, normed_ref, heads):
+    rows, width = q_ref.shape[1:]
     bound = bound_ref[...]
     raw = f_ref[0]
-    forget = bound + (1.0 - bound) * jax.nn.sigmoid(raw)
-    keyvec = (1.0 - bound) * jax.nn.sigmoid(-raw)
-    query = q_ref[0] * jax.nn.sigmoid(q_ref[0])
-    forget_t, keyvec_t, query_t = forget.T, keyvec.T, query.T
+    forget = split(bound + (1.0 - bound) * jax.nn.sigmoid(raw))
+    keyvec = split((1.0 - bound) * jax.nn.sigmoid(-raw))
+    query = split(q_ref[0] * jax.nn.sigmoid(q_ref[0]))
+    values = split(v_ref[0])
+    left = jnp.concatenate([*forget, *keyvec, keyvec[0], *query], axis=0).T.astype(BF16)
+    one, nil = jnp.ones((rows, width), F32), jnp.zeros((rows, width), F32)
+    right = jnp.concatenate(
+        [
+            jnp.concatenate([one, one, nil, nil, nil, nil, nil], axis=0),
+            jnp.concatenate([nil, nil, values[0], values[0], values[1], nil, nil], axis=0),
+            jnp.concatenate([nil, nil, nil, nil, nil, one, one], axis=0),
+        ],
+        axis=1,
+    ).astype(BF16)
+    owner = lax.rem(lax.broadcasted_iota(jnp.int32, right.shape, 0), rows)
     for s in range(rows):
-        new = (
-            forget_t[:, s : s + 1] * state_ref[s, 0]
-            + keyvec_t[:, s : s + 1] * v_ref[0, s : s + 1, :]
-        )
+        mask = jnp.where(owner == s, 1.0, 0.0).astype(BF16)
+        wide = jnp.dot(left, right * mask, preferred_element_type=F32)
+        new = wide[:, :width] * state_ref[s, 0] + wide[:, width : 2 * width]
         new_ref[s, 0] = new
-        head = jnp.sum(query_t[:, s : s + 1] * new, axis=0, keepdims=True)
-        inverse = lax.rsqrt(jnp.mean(head * head, axis=1, keepdims=True) + EPS)
-        gate = g_ref[0, s : s + 1, :]
-        normed_ref[s : s + 1, :] = head * inverse * gain_ref[...] * (gate * jax.nn.sigmoid(gate))
+        heads[s : s + 1, :] = jnp.sum(wide[:, 2 * width :] * new, axis=0, keepdims=True)
+    head = heads[...]
+    inverse = lax.rsqrt(jnp.mean(head * head, axis=1, keepdims=True) + EPS)
+    gate = g_ref[0]
+    normed_ref[...] = head * inverse * gain_ref[...] * (gate * jax.nn.sigmoid(gate))
 
 
 def mix_kernel(
     n_kv, n_tp, features,
     normed_ref, x_ref, gain_ref, w_mix, w_gate, w_up, w_down,
     out_ref,
-    mix_w, gate_w, down_w, normed16, heads, terms, terms_in, mixed, blocks, scaled,
-    squares, squares_in, parts, landed, hidden, hiddens, downs, downs_in,
+    mix_w, gate_w, down_w, normed16, heads, terms, terms_pair, terms_out, terms_in, mixed, blocks, scaled,
+    squares, squares_in, parts, landed, hidden, hiddens, downs, downs_pair, downs_out, downs_in,
     w_sem, n_send, n_recv, t_send, t_recv, m_send, m_recv, s_send, s_recv,
     g_send, g_recv, h_send, h_recv, d_send, d_recv,
 ):
@@ -165,7 +209,8 @@
     kv, kv_peers = ring("kv", n_kv)
     tp, tp_peers = ring("tp", n_tp)
     own = pl.ds(pl.multiple_of(kv * local, local), local)
-    greet((("kv", kv_peers), ("tp", tp_peers)))
+    near = pairs(n_tp)[3]
+    greet((("kv", kv_peers), ("tp", [near] + tp_peers[1::2])))
 
     pending = []
     copies = [
@@ -184,43 +229,44 @@
     while n_tp % group:
         group -= 1
 
-    def scatter(left, weight, sums, sums_in, send, recv):
+    me, core, chip, partner, half = pairs(n_tp)
+
+    def reduce_pairs(base, left, weight, sums, pair_in, joined, sums_in, send, recv):
         for t in range(0, n_tp, group):
             part = jnp.dot(
                 left[...], weight[:, t * width : (t + group) * width], preferred_element_type=F32
             ).astype(BF16)
             for j in range(group):
-                sums[t + j] = part[:, j * width : (j + 1) * width]
-        out = [
-            remote(sums.at[peer], sums_in.at[i], send.at[i], recv.at[i], "tp", peer)
-            for i, peer in enumerate(tp_peers)
-        ]
-        for copy in out:
+                sums[(t + j) % 2, (t + j) // 2] = part[:, j * width : (j + 1) * width]
+        first = remote(sums.at[1 - core], pair_in, send.at[0], recv.at[0], "tp", partner)
+        first.start()
+        first.wait_recv()
+
+        def pair_sum(place):
+            mine = sums[pl.ds(core, 1), pl.ds(place, 1)][0, 0].astype(F32)
+            return mine + pair_in[pl.ds(place, 1)][0].astype(F32)
+
+        out = [first]
+        for i in range(1, half):
+            joined[i - 1] = pair_sum(lax.rem(chip + i, half)).astype(BF16)
+            copy = remote(
+                joined.at[i - 1], sums_in.at[i - 1], send.at[i], recv.at[i],
+                "tp", lax.rem(me + 2 * i, n_tp),
+            )
             copy.start()
-        return out
-
-    def collect(base, sums, sums_in, out):
-        total = base + sums[pl.ds(tp, 1)][0].astype(F32)
-        for copy in out:
-            copy.wait_recv()
-        for i in range(n_tp - 1):
-            total = total + sums_in[i].astype(F32)
+            out.append(copy)
+        total = base + pair_sum(chip)
+        for i in range(1, half):
+            out[i].wait_recv()
+            total = total + sums_in[i - 1].astype(F32)
+        pending.extend(out)
         return total.astype(BF16)
 
-    copies = scatter(heads, mix_w, terms, terms_in, t_send, t_recv)
-    pending += copies
-    mixed[...] = collect(x_ref[...].astype(F32), terms, terms_in, copies)
-
-    copies = [
-        remote(mixed, blocks.at[tp], m_send.at[i], m_recv.at[i], "tp", peer)
-        for i, peer in enumerate(tp_peers)
-    ]
-    for copy in copies:
-        copy.start()
-    pending += copies
-    blocks[pl.ds(tp, 1)] = mixed[...][None]
-    for copy in copies:
-        copy.wait_recv()
+    mixed[...] = reduce_pairs(
+        x_ref[...].astype(F32), heads, mix_w, terms, terms_pair, terms_out, terms_in, t_send, t_recv
+    )
+
+    pending += gather_pairs(n_tp, mixed, blocks, m_send, m_recv)
     squares[...] = scale_block(blocks, gain_ref, scaled, n_tp, width)
     square_copies = [
         remote(
@@ -278,9 +324,9 @@
     loads[3].wait()
     for copy in copies:
         copy.wait_recv()
-    copies = scatter(hiddens, down_w, downs, downs_in, d_send, d_recv)
-    pending += copies
-    out_ref[...] = collect(mixed[...].astype(F32), downs, downs_in, copies)
+    out_ref[...] = reduce_pairs(
+        mixed[...].astype(F32), hiddens, down_w, downs, downs_pair, downs_out, downs_in, d_send, d_recv
+    )
     for copy in pending:
         copy.wait_send()
 
@@ -303,6 +349,7 @@
     local, heads, dk, dv = state.shape
     units = w_gate.shape[1]
     features = depth * n_kv
+    half = n_tp // 2
     dma = pltpu.SemaphoreType.DMA
 
     raw = pl.pallas_call(
@@ -346,6 +393,7 @@
             pl.BlockSpec((rows, 1, dk, dv), lambda h, s: (s, h, 0, 0)),
             pl.BlockSpec((rows, dv), lambda h, s: (s, h)),
         ),
+        scratch_shapes=[pltpu.VMEM((rows, dv), F32)],
         name="state",
     )(raw, raw, raw, raw, lower_bound.reshape(1, hid), head_gain.reshape(1, dv), state)
 
@@ -360,8 +408,10 @@
             pltpu.VMEM(w_down.shape, BF16),
             pltpu.VMEM((local, hid), BF16),
             pltpu.VMEM((seqs, hid), BF16),
-            pltpu.VMEM((n_tp, seqs, width), BF16),
-            pltpu.VMEM((n_tp - 1, seqs, width), BF16),
+            pltpu.VMEM((2, half, seqs, width), BF16),
+            pltpu.VMEM((half, seqs, width), BF16),
+            pltpu.VMEM((half - 1, seqs, width), BF16),
+            pltpu.VMEM((half - 1, seqs, width), BF16),
             pltpu.VMEM((seqs, width), BF16),
             pltpu.VMEM((n_tp, seqs, width), BF16),
             pltpu.VMEM((seqs, depth), BF16),
@@ -371,8 +421,10 @@
             pltpu.VMEM((n_kv - 1, 2, local, units), BF16),
             pltpu.VMEM((local, units), BF16),
             pltpu.VMEM((seqs, units), BF16),
-            pltpu.VMEM((n_tp, seqs, width), BF16),
-            pltpu.VMEM((n_tp - 1, seqs, width), BF16),
+            pltpu.VMEM((2, half, seqs, width), BF16),
+            pltpu.VMEM((half, seqs, width), BF16),
+            pltpu.VMEM((half - 1, seqs, width), BF16),
+            pltpu.VMEM((half - 1, seqs, width), BF16),
             dma((4,)),
             dma((n_kv - 1,)), dma((n_kv - 1,)),
             dma((n_tp - 1,)), dma((n_tp - 1,)),

time: 89.2 us -> 77.3 us (0.87)
  Pallas kernels: 86.3 us -> 74.7 us
    pallas_call x1, Pallas kernels: 19.5 us -> 11.4 us  [body(): pl.pallas_call(state_kernel, grid=(heads, local // rows), out_shape=(jax....]
    pallas_call x1, Pallas kernels: 22 us -> 19.7 us  [body(): pl.pallas_call(functools.partial(project_kernel, n_kv, n_tp, features), o...]
    pallas_call x1, Pallas kernels: 44.8 us -> 43.6 us  [body(): pl.pallas_call(functools.partial(mix_kernel, n_kv, n_tp, features), out_s...]
where the time goes in v2:
time: 77.3 us; the launch traced here: 76.8 us
  Pallas kernels  74.7 us (97%)
  local copies, waits for them, and re-layouts  1.38 us (2%)
    pallas_call x1, Pallas kernels, body(): pl.pallas_call(functools.partial(mix_kernel, n_kv, n_tp, features), out_s...  43.6 us
    pallas_call x1, Pallas kernels, body(): pl.pallas_call(functools.partial(project_kernel, n_kv, n_tp, features), o...  19.7 us
    pallas_call x1, Pallas kernels, body(): pl.pallas_call(state_kernel, grid=(heads, local // rows), out_shape=(jax....  11.4 us

profile of v2, /device:TPU:0, one launch (start us, length us, event | category | flops | bytes accessed | tf_op | source)
XLA Modules:
  0.0 76.8 jit_solution(13784595635102939860)
XLA Ops:
  0.6 19.7 %project.1.q_ref.f_ref.v_ref.g_ref = f32[4,32,512]{2,1,0:T(8,128)} custom-call(bf16[128,128]{1,0:T(8,128)(2,1)} %x_ref.3, f32[1,1024]{1,0:T(1,128)} %bitcast.8, bf16[1024,512]{1,0:T(8,128)(2,1)} %wq.1, bf16[1024,512]{1,0:T(8,128)(2,1)} %wf.1, bf16[1024,512]{1,0:T(8,128)(2,1)} %wi.1, bf16[1024,512]{1,0:T(8,128)(2,1)} %wo.1), custom_call_target="tpu_custom_call" | custom-call | tf_op jit(solution)/shard_map/project/pallas_call | solution.py:355
  20.4 11.4 %state.1 = (f32[32,4,128,128]{3,2,1,0:T(8,128)}, f32[32,512]{1,0:T(8,128)}) custom-call(f32[4,32,512]{2,1,0:T(8,128)} %project.1.q_ref.f_ref.v_ref.g_ref, f32[4,32,512]{2,1,0:T(8,128)} %project.1.q_ref.f_ref.v_ref.g_ref, f32[4,32,512]{2,1,0:T(8,128)} %project.1.q_ref.f_ref.v_ref.g_ref, f32[4,32,512]{2,1,0:T(8,128)} %project.1.q_ref.f_ref.v_ref.g_ref, ...), custom_call_target="tpu_custom_call" | custom-call | tf_op jit(solution)/shard_map/state/pallas_call | solution.py:379
  31.8 43.6 %mix.1 = bf16[128,128]{1,0:T(8,128)(2,1)} custom-call(f32[32,512]{1,0:T(8,128)} %get-tuple-element.4.normed_ref, bf16[128,128]{1,0:T(8,128)(2,1)} %x_ref.3, f32[1,1024]{1,0:T(1,128)} %bitcast.9, bf16[512,1024]{1,0:T(8,128)(2,1)} %w_mix.1, bf16[1344,1024]{1,0:T(8,128)(2,1)} %bitcast.6, bf16[1344,1024]{1,0:T(8,128)(2,1)} %bitcast.7, bf16[1344,1024]{1,0:T(8,128)(2,1)} %w_down.1), custom_call_target="tpu_custom_call" | custom-call | tf_op jit(solution)/shard_map/mix/pallas_call | solution.py:400
  75.4 1.4 %copy.17 = bf16[128,128]{1,0:T(8,128)(2,1)} copy(bf16[128,128]{1,0:T(8,128)(2,1)} %mix.1) | data formatting | bytes 65536
